TPU v7x, 256 devices: a whole 4x4x8 slice. The times are simulated.
256 devices in a mesh: ep: 64 (over z, y, core), tp: 4 (over x).
Axes of the slice: x: 4, y: 4, z: 8, core: 2. Of those that a mesh axis runs over, the one named last changes fastest.
Arguments:
- first_input: bfloat16 [32768, 2048], P('ep'), may hold values from -120 to 120
- first_gain: bfloat16 [2048], replicated, may hold values from 0.099609375 to 1.8984375
- pool_inward: bfloat16 [2048, 1024], P(None, 'tp'), may hold values from -0.125 to 0.125
- pool_mixing: bfloat16 [4, 256, 256], P('tp'), may hold values from -0.375 to 0.375
- pool_scale: bfloat16 [1024], P('tp'), may hold values from 0.099609375 to 1.8984375
- pool_outward: bfloat16 [1024, 2048], P('tp'), may hold values from -0.1875 to 0.1875
- second_input: bfloat16 [16384, 2048], P('ep'), may hold values from -120 to 120
- second_gain: bfloat16 [2048], replicated, may hold values from 0.099609375 to 1.8984375
- route_ids: int32 [16384, 2], P('ep'), may hold values from 0 to 31, all different within a row; in each aligned block of 256 rows (0 to 255, 256 to 511, ...) at most 18 rows name the same one
- route_logits: float32 [16384, 2], P('ep'), may hold values from -6 to 6
- expert_gate: bfloat16 [64, 2048, 2048], P('ep', None, 'tp'), may hold values from -0.125 to 0.125
- expert_up: bfloat16 [64, 2048, 2048], P('ep', None, 'tp'), may hold values from -0.125 to 0.125
- expert_down: bfloat16 [64, 2048, 2048], P('ep', 'tp'), may hold values from -0.09375 to 0.09375
Outputs:
- first_out: bfloat16 [32768, 2048], P('ep', 'tp')
- second_out: bfloat16 [16384, 2048], P('ep', 'tp')
Inputs may be any that keep to these rules, and one draw needn't show every extreme that they name: `route_ids`: each row names two different experts. In each aligned block of 256 rows (the rows of one index of ep) no expert is named by more than 18 rows, and in some blocks one expert is named by exactly 18 rows.
All inputs are finite; a program needn't handle non-finite values.
Results may differ from a plain program's by a relative error of at most 0.012.
Values may be sent and summed in bfloat16 or wider, within the bound.
No kernel may reach another device: no remote copies, remote signals or barrier semaphores. Data moves between devices by JAX's collectives and lax.ppermute only.
A program may use at most 64 MiB of HBM per device.

v0:
```python
import jax
import jax.numpy as jnp
from jax import lax
from jax.sharding import PartitionSpec as P

epsilon = 1e-06


def from_behind(value, axis, steps):
    count = lax.axis_size(axis)
    leading, last = (max(0, -steps), min(count, count - steps))
    return lax.ppermute(value, axis, [(source, source + steps) for source in range(leading, last)])


def rms_scaled(values, weights):
    widened = values.astype(jnp.float32)
    inverse = lax.rsqrt(jnp.mean(widened * widened, axis=-1, keepdims=True) + epsilon)
    return (widened * inverse * weights.astype(jnp.float32)).astype(jnp.bfloat16)


def window_means(channels, length, offset):
    row_count = channels.shape[0] - 15
    summed = jnp.zeros((row_count, channels.shape[1]), jnp.float32)
    for lookback in range(16):
        summed = summed + jnp.where(
            lookback < length, channels[15 - lookback : 15 - lookback + row_count], 0.0
        )
    positions = offset + jnp.arange(row_count, dtype=jnp.int32)
    counts = jnp.minimum(positions + 1, length).astype(jnp.float32)
    return summed / counts[:, None]


def slot_positions(block_ids, expert_count, capacity):
    flattened = block_ids.reshape(-1)
    onehot = (flattened[:, None] == jnp.arange(expert_count, dtype=jnp.int32)[None, :]).astype(
        jnp.int32
    )
    running = jnp.cumsum(onehot, axis=0, dtype=jnp.int32) - 1
    slot_numbers = jnp.sum(onehot * running, axis=1)
    return flattened * capacity + slot_numbers


def expert_output(gate_sum, up_sum, down_rows):
    hidden = (jax.nn.silu(gate_sum) * up_sum).astype(jnp.bfloat16)
    return jnp.dot(hidden, down_rows, preferred_element_type=jnp.float32)


def local(
    first_input,
    first_gain,
    pool_inward,
    pool_mixing,
    pool_scale,
    pool_outward,
    second_input,
    second_gain,
    route_ids,
    route_logits,
    expert_gate,
    expert_up,
    expert_down,
):
    tensor_parts = lax.axis_size("tp")
    expert_count = lax.axis_size("ep") // 2
    model_width = first_input.shape[1]
    quarter_width = model_width // tensor_parts
    normed_first = rms_scaled(first_input, first_gain)
    pooled_in = jnp.dot(normed_first, pool_inward, preferred_element_type=jnp.float32).astype(
        jnp.bfloat16
    )
    halo_rows = from_behind(pooled_in[-15:], "ep", 1)
    extended = jnp.concatenate([halo_rows, pooled_in], axis=0).astype(jnp.float32)
    window = jnp.left_shift(jnp.int32(2), lax.axis_index("tp"))
    sequence_start = lax.axis_index("ep") * first_input.shape[0]
    means = window_means(extended, window, sequence_start)
    mixed = (means - pooled_in.astype(jnp.float32)).astype(jnp.bfloat16)
    pooled = (
        jnp.dot(mixed, pool_mixing[0], preferred_element_type=jnp.float32)
        * pool_scale.astype(jnp.float32)
    ).astype(jnp.bfloat16)
    mixer_term = jnp.dot(pooled, pool_outward, preferred_element_type=jnp.float32)
    normed_second = rms_scaled(second_input, second_gain)
    row_count = second_input.shape[0]
    capacity = 2 * row_count * 9 // (8 * expert_count)
    positions = slot_positions(route_ids, expert_count, capacity)
    repeated = jnp.repeat(normed_second, 2, axis=0)
    repeated = lax.dynamic_slice_in_dim(
        repeated, lax.axis_index("tp") * quarter_width, quarter_width, 1
    )
    send_width = repeated.shape[1]
    buffer = (
        jnp.zeros((expert_count * capacity, send_width), jnp.bfloat16).at[positions].set(repeated)
    )
    paired = jnp.broadcast_to(
        buffer.reshape(expert_count, 1, capacity, send_width),
        (expert_count, 2, capacity, send_width),
    ).reshape(2 * expert_count, capacity, send_width)
    arrived = lax.all_to_all(paired, "ep", split_axis=0, concat_axis=0, tiled=True)
    flattened = arrived.reshape(-1, quarter_width)
    portion = lax.all_gather(flattened, "tp", axis=1, tiled=True)
    gate_rows = expert_gate[0]
    up_rows = expert_up[0]
    gate_sum = jnp.dot(portion, gate_rows, preferred_element_type=jnp.float32)
    up_sum = jnp.dot(portion, up_rows, preferred_element_type=jnp.float32)
    flat_term = expert_output(gate_sum, up_sum, expert_down[0])
    first_summed, expert_summed = (
        lax.psum_scatter(
            mixer_term.astype(jnp.bfloat16), "tp", scatter_dimension=1, tiled=True
        ).astype(jnp.float32),
        lax.psum_scatter(
            flat_term.astype(jnp.bfloat16), "tp", scatter_dimension=1, tiled=True
        ).astype(jnp.float32),
    )
    first_out = first_summed.astype(jnp.bfloat16)
    half_out = expert_summed.astype(jnp.bfloat16).reshape(2 * expert_count, capacity, quarter_width)
    returned = lax.all_to_all(half_out, "ep", split_axis=0, concat_axis=0, tiled=True)
    route_out = jnp.sum(
        returned.reshape(expert_count, 2, capacity, quarter_width).astype(jnp.float32), axis=1
    ).reshape(-1, quarter_width)
    picked = route_out[positions].reshape(row_count, 2, quarter_width)
    shares = jax.nn.sigmoid(route_logits - route_logits[:, ::-1])
    second_out = jnp.sum(picked * shares[:, :, None], axis=1).astype(jnp.bfloat16)
    return (first_out, second_out)


def solution(mesh):
    placed = (
        P("ep", None),
        P(),
        P(None, "tp"),
        P("tp", None, None),
        P("tp"),
        P("tp", None),
        P("ep", None),
        P(),
        P("ep", None),
        P("ep", None),
        P("ep", None, "tp"),
        P("ep", None, "tp"),
        P("ep", "tp", None),
    )
    return jax.shard_map(
        local, mesh=mesh, in_specs=placed, out_specs=(P("ep", "tp"), P("ep", "tp")), check_vma=False
    )
```

profile of v0, /device:TPU:1, one launch (start us, length us, event | category | flops | bytes accessed | tf_op | source)
XLA Modules:
  0.0 273.8 jit_solution(5216356019160819248)
XLA Ops:
  7.2 1.0 copy.17
  9.2 1.2 reduce-window.6
  11.7 1.5 fusion.4
  13.5 2.6 broadcast_in_dim.44
  16.1 4.1 %reshape.103 = bf16[512,2048]{1,0:T(8,128)(2,1)} reshape(bf16[256,2,2048]{2,1,0:T(2,128)(2,1)} %broadcast_in_dim.44) | data formatting | bytes 4194304 | tf_op jit(solution)/shard_map/reshape | solution.py:86
  20.4 3.0 %scatter_custom_fusion = bf16[576,512]{1,0:T(8,128)(2,1)S(1)} fusion(s32[512]{0:T(512)S(1)} %bitcast.41, bf16[512,2048]{1,0:T(8,128)(2,1)} %reshape.103, s32[]{:T(128)} %constant.31.clone.1, s32[]{:T(128)S(6)} %select_n.145, bf16[]{:T(256)} %constant.27.clone.1), kind=kCustom, calls=%fused_computation.61 | custom fusion | bytes 1115140 | tf_op jit(solution)/shard_map/scatter | solution.py:92
  23.7 52.1 %all_to_all.10 = bf16[64,18,512]{2,1,0:T(8,128)(2,1)} all-to-all(bf16[64,18,512]{2,1,0:T(8,128)(2,1)S(1)} %bitcast.40), channel_id=1, replica_groups=mesh['ep'=64,'tp'=4] {'ep'}, dimensions={0} | all-to-all | bytes 2359296 | tf_op jit(solution)/shard_map/all_to_all | solution.py:98
  75.8 3.1 %reshape.105 = bf16[1152,512]{1,0:T(8,128)(2,1)} reshape(bf16[64,18,512]{2,1,0:T(8,128)(2,1)} %all_to_all.10) | data formatting | bytes 2359296 | tf_op jit(solution)/shard_map/reshape | solution.py:99
  79.1 51.9 %all-gather.2.cloned.1.call-done = bf16[1152,2048]{1,0:T(8,128)(2,1)} async-done(((bf16[1152,512]{1,0:T(8,128)(2,1)}), bf16[1152,2048]{1,0:T(8,128)(2,1)}) %all-gather.2.cloned.1.call-update) | async-done | bytes 4718608 | tf_op jit(solution)/shard_map/all_gather | solution.py:100
  131.0 7.0 %fusion.11 = f32[1152,512]{1,0:T(8,128)} fusion(bf16[1152,2048]{1,0:T(8,128)(2,1)} %all-gather.2.cloned.1.call-done, bf16[1,2048,512]{2,1,0:T(8,128)(2,1)} %param.23), kind=kOutput, calls=%fused_computation.20 | convolution fusion | flops 2415919104 | bytes 9175040 | tf_op jit(solution)/shard_map/dot_general | solution.py:103
  138.0 11.0 %convolution_convert_fusion = bf16[1152,2048]{1,0:T(8,128)(2,1)} fusion(bf16[1,512,2048]{2,1,0:T(8,128)(2,1)S(1)} %copy-done, bf16[1152,2048]{1,0:T(8,128)(2,1)} %all-gather.2.cloned.1.call-done, f32[1152,512]{1,0:T(8,128)} %fusion.11, bf16[1,2048,512]{2,1,0:T(8,128)(2,1)} %param.24), kind=kOutput, calls=%fused_computation.2 | convolution fusion | flops 4837736448 | bytes 15990784 | tf_op jit(solution)/shard_map/dot_general | solution.py:45
  149.7 2.2 fusion
  152.0 2.0 fusion.15
  154.1 3.8 %collective-permute-start = (bf16[15,256]{1,0:T(8,128)(2,1)S(1)}, bf16[15,256]{1,0:T(8,128)(2,1)S(1)}, u32[]{:S(2)}, u32[]{:S(2)}) collective-permute-start(bf16[15,256]{1,0:T(8,128)(2,1)S(1)} %slice.78), channel_id=1, source_target_pairs={{0,4},{4,8},{8,12},{12,16},{16,20},{20,24},{24,28},{28,32},{32,36}... | collective-permute-start | bytes 23048 | tf_op jit(solution)/shard_map/ppermute | solution.py:12
  158.7 4.7 %convolution_convert_fusion.1 = bf16[512,2048]{1,0:T(8,128)(2,1)} fusion(bf16[256,2048]{1,0:T(8,128)(2,1)} %param.18, f32[256]{0:T(256)S(1)} %convert_element_type.78, bf16[512,256]{1,0:T(8,128)(2,1)S(1)} %fusion.15, f32[527,256]{1,0:T(8,128)S(1)} %maximum_convert_fusion, f32[512]{0:T(512)S(1)} %minimum_convert_fusion, pred[]{:T(512)S(6)} %gt.63, ...), kind=kOutput, calls=%fused_computation.10 | convolution fusion | flops 609878016 | bytes 11930640 | tf_op jit(solution)/shard_map/dot_general | solution.py:81
  163.5 40.0 %reduce-scatter.5.cloned.1.call-done = bf16[1152,512]{1,0:T(8,128)(2,1)} async-done(((bf16[1152,2048]{1,0:T(8,128)(2,1)}), bf16[1152,512]{1,0:T(8,128)(2,1)}) %reduce-scatter.5.cloned.1.call-update) | async-done | bytes 1179664 | tf_op jit(solution)/shard_map/reduce_scatter | solution.py:110
  203.4 3.0 %reshape.106 = bf16[64,18,512]{2,1,0:T(8,128)(2,1)} reshape(bf16[1152,512]{1,0:T(8,128)(2,1)} %reduce-scatter.5.cloned.1.call-done) | data formatting | bytes 2359296 | tf_op jit(solution)/shard_map/reshape | solution.py:115
  206.5 11.1 %all-to-all-start.1 = ((bf16[64,18,512]{2,1,0:T(8,128)(2,1)}), bf16[64,18,512]{2,1,0:T(8,128)(2,1)}, u32[]{:S(2)}, u32[]{:S(2)}) async-start(bf16[64,18,512]{2,1,0:T(8,128)(2,1)} %reshape.106), calls=%async_computation.3 | async-start | bytes 3145728 | tf_op jit(solution)/shard_map/all_to_all | solution.py:116
  217.8 38.7 %all-to-all-done.1 = bf16[64,18,512]{2,1,0:T(8,128)(2,1)} async-done(((bf16[64,18,512]{2,1,0:T(8,128)(2,1)}), bf16[64,18,512]{2,1,0:T(8,128)(2,1)}, u32[]{:S(2)}, u32[]{:S(2)}) %all-to-all-start.1) | async-done | bytes 1179680 | tf_op jit(solution)/shard_map/all_to_all | solution.py:116
  256.5 3.0 %convert_reduce_fusion = f32[32,18,512]{2,1,0:T(8,128)} fusion(bf16[64,18,512]{2,1,0:T(8,128)(2,1)} %all-to-all-done.1), kind=kLoop, calls=%fused_computation.9 | loop fusion | flops 884736 | bytes 2359296 | tf_op jit(solution)/shard_map/reduce_sum | solution.py:117
  259.5 1.5 reshape.107
  261.1 2.3 gather_fusion
  263.4 1.8 reshape.108
  265.3 2.1 multiply_reduce_fusion
  (48 shorter events, 5.0 us)
Async XLA Ops:
  7.2 130.9 %copy-start = (bf16[1,512,2048]{2,1,0:T(8,128)(2,1)S(1)}, bf16[1,512,2048]{2,1,0:T(8,128)(2,1)}, u32[]{:S(2)}) copy-start(bf16[1,512,2048]{2,1,0:T(8,128)(2,1)} %param.25) | copy-start | bytes 6291460
  7.2 6.0 %copy-start.1 = (bf16[256,2048]{1,0:T(8,128)(2,1)S(1)}, bf16[256,2048]{1,0:T(8,128)(2,1)}, u32[]{:S(2)}) copy-start(bf16[256,2048]{1,0:T(8,128)(2,1)} %param.19) | copy-start | bytes 3145732
  7.2 123.8 %all-gather.2.cloned.1.call-start = ((), (), s32[]{:S(2)}) async-start(), calls=%async_computation.5 | async-start | bytes 5898240 | tf_op jit(solution)/shard_map/all_gather | solution.py:100
  78.9 124.5 %reduce-scatter.5.cloned.1.call-start = ((), (), s32[]{:S(2)}) async-start(), calls=%async_computation.6 | async-start | bytes 5898240 | tf_op jit(solution)/shard_map/reduce_scatter | solution.py:110
  149.0 0.7 copy-start.4
  149.1 118.2 %reduce-scatter.3.cloned.1.call-start = ((), (), s32[]{:S(2)}) async-start(), calls=%async_computation.4 | async-start | bytes 2621440 | tf_op jit(solution)/shard_map/reduce_scatter | solution.py:107
  149.7 2.2 copy-start.2
  152.0 6.0 %copy-start.6 = (bf16[256]{0:T(256)(128)(2,1)S(1)}, bf16[256]{0:T(256)(128)(2,1)}, u32[]{:S(2)}) copy-start(bf16[256]{0:T(256)(128)(2,1)} %param.17) | copy-start | bytes 1540
  152.0 6.7 %copy-start.5 = (bf16[1,256,256]{2,1,0:T(8,128)(2,1)S(1)}, bf16[1,256,256]{2,1,0:T(8,128)(2,1)}, u32[]{:S(2)}) copy-start(bf16[1,256,256]{2,1,0:T(8,128)(2,1)} %param.16) | copy-start | bytes 393220
  154.1 4.6 %collective-permute-start = (bf16[15,256]{1,0:T(8,128)(2,1)S(1)}, bf16[15,256]{1,0:T(8,128)(2,1)S(1)}, u32[]{:S(2)}, u32[]{:S(2)}) collective-permute-start(bf16[15,256]{1,0:T(8,128)(2,1)S(1)} %slice.78), channel_id=1, source_target_pairs={{0,4},{4,8},{8,12},{12,16},{16,20},{20,24},{24,28},{28,32},{32,36}... | collective-permute-start | bytes 23048 | tf_op jit(solution)/shard_map/ppermute | solution.py:12
  206.5 11.1 %copy-start.3 = (f32[256,2]{0,1:T(2,128)S(1)}, f32[256,2]{0,1:T(2,128)}, u32[]{:S(2)}) copy-start(f32[256,2]{0,1:T(2,128)} %param.22) | copy-start | bytes 6148
  206.5 50.1 %all-to-all-start.1 = ((bf16[64,18,512]{2,1,0:T(8,128)(2,1)}), bf16[64,18,512]{2,1,0:T(8,128)(2,1)}, u32[]{:S(2)}, u32[]{:S(2)}) async-start(bf16[64,18,512]{2,1,0:T(8,128)(2,1)} %reshape.106), calls=%async_computation.3 | async-start | bytes 3145728 | tf_op jit(solution)/shard_map/all_to_all | solution.py:116
Sparse Core Ops, SparseCore 0:
  79.0 51.9 all-gather.1
  149.2 54.1 reduce-scatter.4
  206.6 32.0 reduce-scatter.2
where the time goes:
time: 275 us; the launch traced here: 274 us
  waiting for transfers between devices  131 us (48%)
  blocking collectives  52.1 us (19%)
  matrix products  24.8 us (9%)
  local copies, waits for them, and re-layouts  24.5 us (9%)
  starting transfers between devices  15.2 us (6%)
  between operations  14 us (5%)
  other arithmetic  11.9 us (4%)
    all_to_all x1, blocking collectives, local(): lax.all_to_all(paired, 'ep', split_axis=0, concat_axis=0, tiled=True)  52.1 us
    all_gather x1, waiting for transfers between devices, local(): portion = lax.all_gather(flattened, 'tp', axis=1, tiled=True)  51.9 us
    reduce_scatter x1, waiting for transfers between devices, local(): lax.psum_scatter(flat_term.astype(jnp.bfloat16), 'tp', scatter_dimension=...  40 us
    all_to_all x1, waiting for transfers between devices, local(): lax.all_to_all(half_out, 'ep', split_axis=0, concat_axis=0, tiled=True)  38.7 us
    all_to_all x1, starting transfers between devices, local(): lax.all_to_all(half_out, 'ep', split_axis=0, concat_axis=0, tiled=True)  11.1 us
    dot_general x1, matrix products, expert_output(): return jnp.dot(hidden, down_rows, preferred_element_type=jnp.float32)  11 us
    dot_general x1, matrix products, local(): gate_sum = jnp.dot(portion, gate_rows, preferred_element_type=jnp.float32)  7.04 us
  transfers between devices with their start and end apart: 5, of which 4 were waited for; matrix products, arithmetic and copies ran while one was open for 8% of the time, Pallas kernels for 0%

commit v1 on v0

v1 whole, which is shorter than its diff:
```python
import jax
import jax.numpy as jnp
from jax import lax
from jax.sharding import Mesh, PartitionSpec as P

epsilon = 1e-06


def from_behind(value, axis, steps):
    count = lax.axis_size(axis)
    leading, last = (max(0, -steps), min(count, count - steps))
    return lax.ppermute(value, axis, [(source, source + steps) for source in range(leading, last)])


def rms_scaled(values, weights):
    widened = values.astype(jnp.float32)
    inverse = lax.rsqrt(jnp.mean(widened * widened, axis=-1, keepdims=True) + epsilon)
    return (widened * inverse * weights.astype(jnp.float32)).astype(jnp.bfloat16)


def window_means(channels, length, offset):
    row_count = channels.shape[0] - 15
    summed = jnp.zeros((row_count, channels.shape[1]), jnp.float32)
    for lookback in range(16):
        summed = summed + jnp.where(
            lookback < length, channels[15 - lookback : 15 - lookback + row_count], 0.0
        )
    positions = offset + jnp.arange(row_count, dtype=jnp.int32)
    counts = jnp.minimum(positions + 1, length).astype(jnp.float32)
    return summed / counts[:, None]


def slot_positions(block_ids, expert_count, capacity):
    flattened = block_ids.reshape(-1)
    onehot = (flattened[:, None] == jnp.arange(expert_count, dtype=jnp.int32)[None, :]).astype(
        jnp.int32
    )
    running = jnp.cumsum(onehot, axis=0, dtype=jnp.int32) - 1
    slot_numbers = jnp.sum(onehot * running, axis=1)
    return flattened * capacity + slot_numbers


def expert_output(gate_sum, up_sum, down_rows):
    hidden = (jax.nn.silu(gate_sum) * up_sum).astype(jnp.bfloat16)
    return jnp.dot(hidden, down_rows, preferred_element_type=jnp.float32)


def local(
    first_input,
    first_gain,
    pool_inward,
    pool_mixing,
    pool_scale,
    pool_outward,
    second_input,
    second_gain,
    route_ids,
    route_logits,
    expert_gate,
    expert_up,
    expert_down,
):
    tensor_parts = lax.axis_size("tp")
    expert_count = lax.axis_size("z") * lax.axis_size("y")
    model_width = first_input.shape[1]
    quarter_width = model_width // tensor_parts
    swap = [(0, 1), (1, 0)]
    gate_other = lax.ppermute(expert_gate[0], "core", swap)
    up_other = lax.ppermute(expert_up[0], "core", swap)
    down_other = lax.ppermute(expert_down[0], "core", swap)
    normed_first = rms_scaled(first_input, first_gain)
    pooled_in = jnp.dot(normed_first, pool_inward, preferred_element_type=jnp.float32).astype(
        jnp.bfloat16
    )
    halo_rows = from_behind(pooled_in[-15:], ("z", "y", "core"), 1)
    extended = jnp.concatenate([halo_rows, pooled_in], axis=0).astype(jnp.float32)
    window = jnp.left_shift(jnp.int32(2), lax.axis_index("tp"))
    sequence_start = lax.axis_index(("z", "y", "core")) * first_input.shape[0]
    means = window_means(extended, window, sequence_start)
    mixed = (means - pooled_in.astype(jnp.float32)).astype(jnp.bfloat16)
    pooled = (
        jnp.dot(mixed, pool_mixing[0], preferred_element_type=jnp.float32)
        * pool_scale.astype(jnp.float32)
    ).astype(jnp.bfloat16)
    mixer_term = jnp.dot(pooled, pool_outward, preferred_element_type=jnp.float32)
    normed_second = rms_scaled(second_input, second_gain)
    row_count = second_input.shape[0]
    capacity = 2 * row_count * 9 // (8 * expert_count)
    positions = slot_positions(route_ids, expert_count, capacity)
    quarter = lax.dynamic_slice_in_dim(
        normed_second, lax.axis_index("tp") * quarter_width, quarter_width, 1
    )
    repeated = jnp.repeat(quarter, 2, axis=0)
    buffer = (
        jnp.zeros((expert_count * capacity, quarter_width), jnp.bfloat16)
        .at[positions]
        .set(repeated)
    ).reshape(expert_count, capacity, quarter_width)
    arrived = lax.all_to_all(buffer, ("z", "y"), split_axis=0, concat_axis=0, tiled=True)
    flattened = arrived.reshape(-1, quarter_width)
    portion = lax.all_gather(flattened, "tp", axis=1, tiled=True)
    flat_term = expert_output(
        jnp.dot(portion, expert_gate[0], preferred_element_type=jnp.float32),
        jnp.dot(portion, expert_up[0], preferred_element_type=jnp.float32),
        expert_down[0],
    ) + expert_output(
        jnp.dot(portion, gate_other, preferred_element_type=jnp.float32),
        jnp.dot(portion, up_other, preferred_element_type=jnp.float32),
        down_other,
    )
    first_out = lax.psum_scatter(
        mixer_term.astype(jnp.bfloat16), "tp", scatter_dimension=1, tiled=True
    )
    expert_summed = lax.psum_scatter(
        flat_term.astype(jnp.bfloat16), "tp", scatter_dimension=1, tiled=True
    )
    half_out = expert_summed.reshape(expert_count, capacity, quarter_width)
    returned = lax.all_to_all(half_out, ("z", "y"), split_axis=0, concat_axis=0, tiled=True)
    route_out = returned.reshape(-1, quarter_width).astype(jnp.float32)
    picked = route_out[positions].reshape(row_count, 2, quarter_width)
    shares = jax.nn.sigmoid(route_logits - route_logits[:, ::-1])
    second_out = jnp.sum(picked * shares[:, :, None], axis=1).astype(jnp.bfloat16)
    return (first_out, second_out)


def solution(mesh):
    split_mesh = Mesh(mesh.devices.reshape(8, 4, 2, 4), ("z", "y", "core", "tp"))
    ep = ("z", "y", "core")
    placed = (
        P(ep, None),
        P(),
        P(None, "tp"),
        P("tp", None, None),
        P("tp"),
        P("tp", None),
        P(ep, None),
        P(),
        P(ep, None),
        P(ep, None),
        P(ep, None, "tp"),
        P(ep, None, "tp"),
        P(ep, "tp", None),
    )
    return jax.shard_map(
        local,
        mesh=split_mesh,
        in_specs=placed,
        out_specs=(P(ep, "tp"), P(ep, "tp")),
        check_vma=False,
    )
```

time: 275 us -> 190 us (0.69)
  waiting for transfers between devices: 131 us -> 75.9 us
  blocking collectives: 52.1 us -> 32.9 us
  local copies, waits for them, and re-layouts: 24.5 us -> 11.5 us
  matrix products: 24.8 us -> 28.7 us
  other arithmetic: 11.9 us -> 8.35 us
    all_gather x1, waiting for transfers between devices: 51.9 us -> 30.8 us  [local(): portion = lax.all_gather(flattened, 'tp', axis=1, tiled=True)]
    all_to_all x1, blocking collectives: 52.1 us -> 32.9 us  [local(): lax.all_to_all(buffer, ('z', 'y'), split_axis=0, concat_axis=0, tiled=True)]
    all_to_all x1, waiting for transfers between devices: 38.7 us -> 20.8 us  [local(): lax.all_to_all(half_out, ('z', 'y'), split_axis=0, concat_axis=0, tiled=T...]
    reduce_scatter x1, waiting for transfers between devices: 40 us -> 23.6 us  [local(): lax.psum_scatter(flat_term.astype(jnp.bfloat16), 'tp', scatter_dimension=...]
    reshape x3, local copies, waits for them, and re-layouts: 8.69 us -> 2.48 us  [the longest x1 2.11 us: local(): half_out = expert_summed.reshape(expert_count, capacity, quarter_width)]
    dot_general x1 -> x2, matrix products: 11 us -> 15.5 us  [expert_output(): return jnp.dot(hidden, down_rows, preferred_element_type=jnp.float32)]
    ppermute x0 -> x3, starting transfers between devices: none -> 3.36 us  [the longest x1 2.85 us: local(): gate_other = lax.ppermute(expert_gate[0], 'core', swap)]
    reduce_sum x1 -> x0, other arithmetic: 3 us -> none  [local(): jnp.sum(returned.reshape(expert_count, 2, capacity, quarter_width).astype...]
  transfers between devices with their start and end apart: 5 -> 8, of which waited for: 4 -> 4; matrix products, arithmetic and copies ran while one was open for 8% -> 15% of each run, Pallas kernels for 0% -> 0%
where the time goes in v1:
time: 190 us; the launch traced here: 188 us
  waiting for transfers between devices  75.9 us (40%)
  blocking collectives  32.9 us (17%)
  matrix products  28.7 us (15%)
  starting transfers between devices  16.9 us (9%)
  between operations  14.1 us (7%)
  local copies, waits for them, and re-layouts  11.5 us (6%)
  other arithmetic  8.35 us (4%)
    all_to_all x1, blocking collectives, local(): lax.all_to_all(buffer, ('z', 'y'), split_axis=0, concat_axis=0, tiled=True)  32.9 us
    all_gather x1, waiting for transfers between devices, local(): portion = lax.all_gather(flattened, 'tp', axis=1, tiled=True)  30.8 us
    reduce_scatter x1, waiting for transfers between devices, local(): lax.psum_scatter(flat_term.astype(jnp.bfloat16), 'tp', scatter_dimension=...  23.6 us
    all_to_all x1, waiting for transfers between devices, local(): lax.all_to_all(half_out, ('z', 'y'), split_axis=0, concat_axis=0, tiled=T...  20.8 us
    dot_general x2, matrix products, expert_output(): return jnp.dot(hidden, down_rows, preferred_element_type=jnp.float32)  15.5 us
    all_to_all x1, starting transfers between devices, local(): lax.all_to_all(half_out, ('z', 'y'), split_axis=0, concat_axis=0, tiled=T...  9.57 us
    dot_general x1, matrix products, local(): jnp.dot(portion, expert_gate[0], preferred_element_type=jnp.float32)  4.89 us
    dot_general x1, matrix products, local(): jnp.dot(portion, gate_other, preferred_element_type=jnp.float32)  3.97 us
  transfers between devices with their start and end apart: 8, of which 4 were waited for; matrix products, arithmetic and copies ran while one was open for 15% of the time, Pallas kernels for 0%

profile of v1, /device:TPU:1, one launch (start us, length us, event | category | flops | bytes accessed | tf_op | source)
XLA Modules:
  0.0 188.3 jit_solution(17867324479856150440)
XLA Ops:
  7.3 3.0 %convert_element_type.81 = f32[256,2048]{1,0:T(8,128)} convert(bf16[256,2048]{1,0:T(8,128)(2,1)} %param.19) | non-fusion elementwise | flops 524288 | bytes 3145728 | tf_op jit(solution)/shard_map/convert_element_type | solution.py:16
  11.1 1.2 fusion.16
  12.7 1.2 reduce-window.6
  14.6 2.6 %scatter_custom_fusion = bf16[576,512]{1,0:T(8,128)(2,1)S(1)} fusion(s32[512]{0:T(512)S(1)} %bitcast.40, bf16[512,512]{1,0:T(8,128)(2,1)S(1)} %reshape.116, bf16[]{:T(256)} %constant.77.clone.1), kind=kCustom, calls=%fused_computation.60 | custom fusion | bytes 589826 | tf_op jit(solution)/shard_map/scatter | solution.py:97
  17.3 32.9 %all_to_all.10 = bf16[32,18,512]{2,1,0:T(8,128)(2,1)S(1)} all-to-all(bf16[32,18,512]{2,1,0:T(8,128)(2,1)S(1)} %reshape.99), channel_id=1, replica_groups=mesh['z'=8,'y'=4,'core'=2,'tp'=4] {'z','y'}, dimensions={0} | all-to-all | bytes 1179648 | tf_op jit(solution)/shard_map/all_to_all | solution.py:99
  50.2 1.0 reshape.100
  51.3 2.9 %collective-permute-start.1 = (bf16[2048,512]{1,0:T(8,128)(2,1)}, bf16[2048,512]{1,0:T(8,128)(2,1)}, u32[]{:S(2)}, u32[]{:S(2)}) collective-permute-start(bf16[2048,512]{1,0:T(8,128)(2,1)} %bitcast.43), channel_id=1, source_target_pairs={{0,4},{4,0},{1,5},{5,1},{2,6},{6,2},{3,7},{7,3},{8,12},{12,8},{9,1... | collective-permute-start | bytes 6291464 | tf_op jit(solution)/shard_map/ppermute | solution.py:68
  54.6 30.8 %all-gather.2.cloned.1.call-done = bf16[576,2048]{1,0:T(8,128)(2,1)} async-done(((bf16[576,512]{1,0:T(8,128)(2,1)}), bf16[576,2048]{1,0:T(8,128)(2,1)}) %all-gather.2.cloned.1.call-update) | async-done | bytes 2359312 | tf_op jit(solution)/shard_map/all_gather | solution.py:101
  85.4 4.9 %fusion.80 = f32[576,512]{1,0:T(8,128)} fusion(bf16[576,2048]{1,0:T(8,128)(2,1)} %all-gather.2.cloned.1.call-done, bf16[1,2048,512]{2,1,0:T(8,128)(2,1)} %param.23), kind=kOutput, calls=%fused_computation.98 | convolution fusion | flops 1207959552 | bytes 5636096 | tf_op jit(solution)/shard_map/dot_general | solution.py:103
  90.3 4.0 %fusion.88 = f32[576,512]{1,0:T(8,128)} fusion(bf16[576,2048]{1,0:T(8,128)(2,1)S(1)} %copy-done.7, bf16[2048,512]{1,0:T(8,128)(2,1)} %collective-permute-done.1), kind=kOutput, calls=%fused_computation.104 | convolution fusion | flops 1207959552 | bytes 5636096 | tf_op jit(solution)/shard_map/dot_general | solution.py:107
  94.3 7.4 %fusion.12 = f32[576,2048]{1,0:T(8,128)} fusion(bf16[576,2048]{1,0:T(8,128)(2,1)S(1)} %copy-done.7, f32[576,512]{1,0:T(8,128)} %fusion.80, bf16[1,512,2048]{2,1,0:T(8,128)(2,1)} %param.25, bf16[1,2048,512]{2,1,0:T(8,128)(2,1)} %param.24), kind=kOutput, calls=%fused_computation.20 | convolution fusion | flops 2417688576 | bytes 12451840 | tf_op jit(solution)/shard_map/dot_general | solution.py:45
  101.7 8.1 %add_convert_fusion = bf16[576,2048]{1,0:T(8,128)(2,1)} fusion(f32[576,2048]{1,0:T(8,128)} %fusion.12, bf16[512,2048]{1,0:T(8,128)(2,1)} %collective-permute-done.3, f32[576,512]{1,0:T(8,128)} %fusion.88, bf16[576,2048]{1,0:T(8,128)(2,1)S(1)} %copy-done.7, bf16[2048,512]{1,0:T(8,128)(2,1)} %collective-permute-done.2), kind=kOutput, calls=%fused_computation.4 | convolution fusion | flops 2420047872 | bytes 14811136 | tf_op jit(solution)/shard_map/dot_general | solution.py:45
  110.5 0.9 copy-done.2
  111.9 0.8 fusion.8
  112.7 3.8 %collective-permute-start = (bf16[15,256]{1,0:T(8,128)(2,1)S(1)}, bf16[15,256]{1,0:T(8,128)(2,1)S(1)}, u32[]{:S(2)}, u32[]{:S(2)}) collective-permute-start(bf16[15,256]{1,0:T(8,128)(2,1)S(1)} %slice.78), channel_id=1, source_target_pairs={{0,4},{4,8},{8,12},{12,16},{16,20},{20,24},{24,28},{28,32},{32,36}... | collective-permute-start | bytes 23048 | tf_op jit(solution)/shard_map/ppermute | solution.py:12
  116.6 0.7 collective-permute-done
  117.4 3.5 %convolution_convert_fusion = bf16[512,2048]{1,0:T(8,128)(2,1)} fusion(bf16[256,2048]{1,0:T(8,128)(2,1)S(1)} %copy-done, f32[256]{0:T(256)S(1)} %convert_element_type.77, bf16[512,256]{1,0:T(8,128)(2,1)S(1)} %fusion.8, f32[527,256]{1,0:T(8,128)S(1)} %maximum_convert_fusion, f32[512]{0:T(512)S(1)} %minimum_convert_fusion, pred[]{:T(512)S(6)} %gt.63, ...), kind=kOutput, calls=%fused_computation.8 | convolution fusion | flops 609878016 | bytes 11930640 | tf_op jit(solution)/shard_map/dot_general | solution.py:85
  120.9 23.6 %reduce-scatter.5.cloned.1.call-done = bf16[576,512]{1,0:T(8,128)(2,1)} async-done(((bf16[576,2048]{1,0:T(8,128)(2,1)}), bf16[576,512]{1,0:T(8,128)(2,1)}) %reduce-scatter.5.cloned.1.call-update) | async-done | bytes 589840 | tf_op jit(solution)/shard_map/reduce_scatter | solution.py:114
  144.5 2.1 %reshape.101 = bf16[32,18,512]{2,1,0:T(8,128)(2,1)} reshape(bf16[576,512]{1,0:T(8,128)(2,1)} %reduce-scatter.5.cloned.1.call-done) | data formatting | bytes 1179648 | tf_op jit(solution)/shard_map/reshape | solution.py:117
  146.6 9.6 %all-to-all-start.1 = ((bf16[32,18,512]{2,1,0:T(8,128)(2,1)}), bf16[32,18,512]{2,1,0:T(8,128)(2,1)S(1)}, u32[]{:S(2)}, u32[]{:S(2)}) async-start(bf16[32,18,512]{2,1,0:T(8,128)(2,1)} %reshape.101), calls=%async_computation.3 | async-start | bytes 1572864 | tf_op jit(solution)/shard_map/all_to_all | solution.py:118
  156.5 20.8 %all-to-all-done.1 = bf16[32,18,512]{2,1,0:T(8,128)(2,1)S(1)} async-done(((bf16[32,18,512]{2,1,0:T(8,128)(2,1)}), bf16[32,18,512]{2,1,0:T(8,128)(2,1)S(1)}, u32[]{:S(2)}, u32[]{:S(2)}) %all-to-all-start.1) | async-done | bytes 589856 | tf_op jit(solution)/shard_map/all_to_all | solution.py:118
  177.4 1.6 gather_fusion
  179.1 0.6 reshape.102
  179.7 2.1 %multiply_reduce_fusion.1 = bf16[256,512]{1,0:T(8,128)(2,1)} fusion(f32[256,2,512]{2,1,0:T(2,128)S(1)} %reshape.102, f32[256,2]{1,0:T(8,128)S(1)} %copy.20), kind=kLoop, calls=%fused_computation.19 | loop fusion | flops 393216 | bytes 1312768 | tf_op jit(solution)/shard_map/reduce_sum | solution.py:122
  (63 shorter events, 4.4 us)
Async XLA Ops:
  7.2 110.2 %copy-start = (bf16[256,2048]{1,0:T(8,128)(2,1)S(1)}, bf16[256,2048]{1,0:T(8,128)(2,1)}, u32[]{:S(2)}) copy-start(bf16[256,2048]{1,0:T(8,128)(2,1)} %param.18) | copy-start | bytes 3145732
  7.2 3.0 %copy-start.1 = (bf16[256,2048]{1,0:T(8,128)(2,1)S(1)}, bf16[256,2048]{1,0:T(8,128)(2,1)}, u32[]{:S(2)}) copy-start(bf16[256,2048]{1,0:T(8,128)(2,1)} %param.19) | copy-start | bytes 3145732
  7.2 78.2 %all-gather.2.cloned.1.call-start = ((), (), s32[]{:S(2)}) async-start(), calls=%async_computation.5 | async-start | bytes 2949120 | tf_op jit(solution)/shard_map/all_gather | solution.py:101
  7.2 3.3 %copy-start.3 = (s32[256,2]{0,1:T(2,128)S(1)}, s32[256,2]{0,1:T(2,128)}, u32[]{:S(2)}) copy-start(s32[256,2]{0,1:T(2,128)} %param.21) | copy-start | bytes 6148
  7.2 3.7 %copy-start.6 = (bf16[2048]{0:T(1024)(128)(2,1)S(1)}, bf16[2048]{0:T(1024)(128)(2,1)}, u32[]{:S(2)}) copy-start(bf16[2048]{0:T(1024)(128)(2,1)} %param.20) | copy-start | bytes 12292
  51.2 93.3 %reduce-scatter.5.cloned.1.call-start = ((), (), s32[]{:S(2)}) async-start(), calls=%async_computation.6 | async-start | bytes 2949120 | tf_op jit(solution)/shard_map/reduce_scatter | solution.py:114
  51.3 39.0 %collective-permute-start.1 = (bf16[2048,512]{1,0:T(8,128)(2,1)}, bf16[2048,512]{1,0:T(8,128)(2,1)}, u32[]{:S(2)}, u32[]{:S(2)}) collective-permute-start(bf16[2048,512]{1,0:T(8,128)(2,1)} %bitcast.43), channel_id=1, source_target_pairs={{0,4},{4,0},{1,5},{5,1},{2,6},{6,2},{3,7},{7,3},{8,12},{12,8},{9,1... | collective-permute-start | bytes 6291464 | tf_op jit(solution)/shard_map/ppermute | solution.py:68
  54.1 47.5 %collective-permute-start.2 = (bf16[2048,512]{1,0:T(8,128)(2,1)}, bf16[2048,512]{1,0:T(8,128)(2,1)}, u32[]{:S(2)}, u32[]{:S(2)}) collective-permute-start(bf16[2048,512]{1,0:T(8,128)(2,1)} %bitcast.44), channel_id=1, source_target_pairs={{0,4},{4,0},{1,5},{5,1},{2,6},{6,2},{3,7},{7,3},{8,12},{12,8},{9,1... | collective-permute-start | bytes 6291464 | tf_op jit(solution)/shard_map/ppermute | solution.py:69
  54.2 47.4 %collective-permute-start.3 = (bf16[512,2048]{1,0:T(8,128)(2,1)}, bf16[512,2048]{1,0:T(8,128)(2,1)}, u32[]{:S(2)}, u32[]{:S(2)}) collective-permute-start(bf16[512,2048]{1,0:T(8,128)(2,1)} %bitcast.45), channel_id=1, source_target_pairs={{0,4},{4,0},{1,5},{5,1},{2,6},{6,2},{3,7},{7,3},{8,12},{12,8},{9,1... | collective-permute-start | bytes 6291464 | tf_op jit(solution)/shard_map/ppermute | solution.py:70
  85.4 4.9 %copy-start.7 = (bf16[576,2048]{1,0:T(8,128)(2,1)S(1)}, bf16[576,2048]{1,0:T(8,128)(2,1)}, u32[]{:S(2)}) copy-start(bf16[576,2048]{1,0:T(8,128)(2,1)} %all-gather.2.cloned.1.call-done) | copy-start | bytes 7077892
  109.8 0.7 copy-start.5
  109.8 1.6 copy-start.2
  109.8 71.9 %reduce-scatter.3.cloned.1.call-start = ((), (), s32[]{:S(2)}) async-start(), calls=%async_computation.4 | async-start | bytes 2621440 | tf_op jit(solution)/shard_map/reduce_scatter | solution.py:111
  110.5 1.4 copy-start.8
  111.9 4.7 %copy-start.10 = (bf16[256]{0:T(256)(128)(2,1)S(1)}, bf16[256]{0:T(256)(128)(2,1)}, u32[]{:S(2)}) copy-start(bf16[256]{0:T(256)(128)(2,1)} %param.17) | copy-start | bytes 1540
  111.9 5.5 %copy-start.9 = (bf16[1,256,256]{2,1,0:T(8,128)(2,1)S(1)}, bf16[1,256,256]{2,1,0:T(8,128)(2,1)}, u32[]{:S(2)}) copy-start(bf16[1,256,256]{2,1,0:T(8,128)(2,1)} %param.16) | copy-start | bytes 393220
  112.7 4.6 %collective-permute-start = (bf16[15,256]{1,0:T(8,128)(2,1)S(1)}, bf16[15,256]{1,0:T(8,128)(2,1)S(1)}, u32[]{:S(2)}, u32[]{:S(2)}) collective-permute-start(bf16[15,256]{1,0:T(8,128)(2,1)S(1)} %slice.78), channel_id=1, source_target_pairs={{0,4},{4,8},{8,12},{12,16},{16,20},{20,24},{24,28},{28,32},{32,36}... | collective-permute-start | bytes 23048 | tf_op jit(solution)/shard_map/ppermute | solution.py:12
  120.9 35.3 %copy-start.4 = (f32[256,2]{0,1:T(2,128)S(1)}, f32[256,2]{0,1:T(2,128)}, u32[]{:S(2)}) copy-start(f32[256,2]{0,1:T(2,128)} %param.22) | copy-start | bytes 6148
  146.6 30.6 %all-to-all-start.1 = ((bf16[32,18,512]{2,1,0:T(8,128)(2,1)}), bf16[32,18,512]{2,1,0:T(8,128)(2,1)S(1)}, u32[]{:S(2)}, u32[]{:S(2)}) async-start(bf16[32,18,512]{2,1,0:T(8,128)(2,1)} %reshape.101), calls=%async_computation.3 | async-start | bytes 1572864 | tf_op jit(solution)/shard_map/all_to_all | solution.py:118
Sparse Core Ops, SparseCore 0:
  51.3 34.0 all-gather.1
  109.9 34.5 reduce-scatter.4
  147.7 31.9 reduce-scatter.2
